TPU v7x, 32 devices: a whole 2x2x4 slice. The times are simulated.
32 devices in a mesh: grp: 2 (over y), fs: 4 (over z), tp: 4 (over x, core).
Axes of the slice: x: 2, y: 2, z: 4, core: 2. Of those that a mesh axis runs over, the one named last changes fastest.
Arguments:
- stream: bfloat16 [8, 128, 2048], P(('grp', 'fs')), parts along dimension 0, may hold values from -6 to 6
- in_gain: float32 [2048], replicated, may hold values from 0.2 to 5
- value_weight: bfloat16 [2048, 1024], P('fs', 'tp'), may hold values from -0.125 to 0.125
- gate_weight: bfloat16 [2048, 1024], P('fs', 'tp'), may hold values from -0.125 to 0.125
- conv_kernel: bfloat16 [31, 1024], P(None, 'tp'), may hold values from -3.6 to 3.6
- conv_gain: float32 [1024], P('tp'), may hold values from 0.1 to 1.9
- conv_shift: float32 [1024], P('tp'), may hold values from -3 to 3
- out_weight: bfloat16 [1024, 2048], P('tp', 'fs'), may hold values from -0.1875 to 0.1875
- norm_gain: float32 [2048], replicated, may hold values from 0.2 to 5
- up_weight: bfloat16 [2048, 8192], P('fs', 'tp'), may hold values from -0.125 to 0.125
- down_weight: bfloat16 [8192, 2048], P('tp', 'fs'), may hold values from -0.0625 to 0.0625
- out_gain: float32 [2048], P('tp'), may hold values from 0.1 to 1.9
Outputs:
- result: bfloat16 [8, 128, 2048], P(('grp', 'fs'), None, 'tp'), parts along dimension 0
There are 2 independent parts, one for each index of `grp`. A program takes and returns all parts, laid end to end along the dimension named above; an argument that names none is the same for every part. Nothing has to cross between parts.
All inputs are finite; a program needn't handle non-finite values.
Results may differ from a plain program's by a relative error of at most 0.02.
Values may be sent and summed in bfloat16 or wider, within the bound.
A program may use at most 64 MiB of HBM per device.

v0:
```python
import jax
import jax.numpy as jnp
from jax import lax
from jax.sharding import PartitionSpec as P

KW = 31


norm_epsilon = 1e-05
residual_scale = 2.0**0.25


def norm_rows(values, gain_vector):
    row_mean = jnp.mean(values, axis=-1, keepdims=True)
    row_var = jnp.mean(jnp.square(values - row_mean), axis=-1, keepdims=True)
    return (values - row_mean) * lax.rsqrt(row_var + norm_epsilon) * gain_vector


def norm_shares(summed, stat_sums, full_width, gain_vector):
    row_mean = stat_sums[0] / full_width
    row_var = stat_sums[1] / full_width - row_mean * row_mean
    return (summed - row_mean[:, None]) * lax.rsqrt(row_var + norm_epsilon)[:, None] * gain_vector


def row_sums(summed):
    return (jnp.sum(summed, axis=1), jnp.sum(summed * summed, axis=1))


def contract(left, turned):
    return lax.dot_general(
        left, turned, (((1,), (1,)), ((), ())), preferred_element_type=jnp.float32
    )


def shards(
    stream,
    in_gain,
    value_weight,
    gate_weight,
    conv_kernel,
    conv_gain,
    conv_shift,
    out_weight,
    norm_gain,
    up_weight,
    down_weight,
    out_gain,
):
    seq_count, seq_length, model_width = stream.shape
    token_count = seq_count * seq_length
    tp_count = lax.axis_size("tp")
    slice_width = model_width // tp_count
    tp_index = lax.axis_index("tp")
    out_turned_shard = out_weight.T
    down_turned_shard = down_weight.T
    value_whole, gate_whole, out_turned, up_whole, down_turned = (
        lax.all_gather(value_weight, "fs", axis=0, tiled=True),
        lax.all_gather(gate_weight, "fs", axis=0, tiled=True),
        lax.all_gather(out_turned_shard, "fs", axis=0, tiled=True),
        lax.all_gather(up_weight, "fs", axis=0, tiled=True),
        lax.all_gather(down_turned_shard, "fs", axis=0, tiled=True),
    )
    normed = norm_rows(
        stream.reshape(token_count, model_width).astype(jnp.float32), in_gain
    ).astype(jnp.bfloat16)
    channels = value_weight.shape[1]
    values = jnp.dot(normed, value_whole, preferred_element_type=jnp.float32)
    gating = jnp.dot(normed, gate_whole, preferred_element_type=jnp.float32)
    gated = (values * jax.nn.sigmoid(gating)).astype(jnp.bfloat16)
    convolved = lax.conv_general_dilated(
        gated.reshape(seq_count, seq_length, channels),
        conv_kernel[:, None, :],
        window_strides=(1,),
        padding=[(KW - 1, 0)],
        dimension_numbers=("NWC", "WIO", "NWC"),
        feature_group_count=channels,
        preferred_element_type=jnp.float32,
    ).reshape(token_count, channels)
    conv_sums = lax.psum(row_sums(convolved), "tp")
    activated = jax.nn.silu(
        norm_shares(convolved, conv_sums, channels * tp_count, conv_gain) + conv_shift
    ).astype(jnp.bfloat16)
    partial_terms = contract(activated, out_turned)
    mixed = lax.psum_scatter(
        partial_terms.astype(jnp.bfloat16), "tp", scatter_dimension=1, tiled=True
    )
    normed_own = lax.dynamic_slice_in_dim(normed, tp_index * slice_width, slice_width, 1)
    gain_own = lax.dynamic_slice_in_dim(norm_gain, tp_index * slice_width, slice_width, 0)
    summed = residual_scale * normed_own.astype(jnp.float32) + mixed.astype(jnp.float32)
    mix_sums = lax.psum(row_sums(summed), "tp")
    settled_own = norm_shares(summed, mix_sums, model_width, gain_own).astype(jnp.bfloat16)
    settled_full = lax.all_gather(settled_own, "tp", axis=1, tiled=True)
    hidden = jnp.square(
        jax.nn.relu(jnp.dot(settled_full, up_whole, preferred_element_type=jnp.float32))
    ).astype(jnp.bfloat16)
    fed_terms = contract(hidden, down_turned)
    fed = lax.psum_scatter(fed_terms.astype(jnp.bfloat16), "tp", scatter_dimension=1, tiled=True)
    final_sum = residual_scale * settled_own.astype(jnp.float32) + fed.astype(jnp.float32)
    out_sums = lax.psum(row_sums(final_sum), "tp")
    result = norm_shares(final_sum, out_sums, model_width, out_gain).astype(jnp.bfloat16)
    return result.reshape(seq_count, seq_length, slice_width)


def solution(mesh):
    in_specs = (
        P(("grp", "fs"), None, None),
        P(),
        P("fs", "tp"),
        P("fs", "tp"),
        P(None, "tp"),
        P("tp"),
        P("tp"),
        P("tp", "fs"),
        P(),
        P("fs", "tp"),
        P("tp", "fs"),
        P("tp"),
    )
    out_specs = P(("grp", "fs"), None, "tp")
    return jax.shard_map(shards, mesh=mesh, in_specs=in_specs, out_specs=out_specs, check_vma=False)
```

profile of v0, /device:TPU:0, one launch (start us, length us, event | category | flops | bytes accessed | tf_op | source)
XLA Modules:
  0.0 465.8 jit_solution(17300026285777350739)
XLA Ops:
  8.8 1.2 convert_reduce_fusion
  10.0 1.3 fusion.11
  11.3 1.4 fusion.13
  12.8 26.9 %all-gather.6.cloned.1.call-done = bf16[2048,256]{1,0:T(8,128)(2,1)} async-done(((bf16[512,256]{1,0:T(8,128)(2,1)}), bf16[2048,256]{1,0:T(8,128)(2,1)}) %all-gather.6.cloned.1.call-update) | async-done | bytes 1048592 | tf_op jit(solution)/shard_map/all_gather | solution.py:57
  39.6 1.5 fusion.33
  41.2 27.4 %all-gather.8.cloned.1.call-done = bf16[2048,256]{1,0:T(8,128)(2,1)} async-done(((bf16[512,256]{1,0:T(8,128)(2,1)}), bf16[2048,256]{1,0:T(8,128)(2,1)}) %all-gather.8.cloned.1.call-update) | async-done | bytes 1048592 | tf_op jit(solution)/shard_map/all_gather | solution.py:58
  68.6 1.5 fusion.7
  70.2 2.2 fusion.32
  72.5 6.1 %all-reduce.2 = (f32[128]{0:T(128)S(1)}, f32[128]{0:T(128)S(1)}) all-reduce(f32[128]{0:T(128)S(1)} %fusion.21, f32[128]{0:T(128)S(1)} %get-tuple-element.21), channel_id=1, replica_groups=mesh['grp'=2,'fs'=4,'tp'=4] {'tp'}, use_global_device_ids=true, to_apply=%region_5.0 | all-reduce | flops 256 | bytes 2048 | tf_op jit(solution)/shard_map/psum | solution.py:79
  78.5 19.0 %all-gather.10.cloned.1.call-done = bf16[2048,256]{0,1:T(8,128)(2,1)} async-done(((bf16[512,256]{0,1:T(8,128)(2,1)}), bf16[2048,256]{0,1:T(8,128)(2,1)}) %all-gather.10.cloned.1.call-update) | async-done | bytes 1048592 | tf_op jit(solution)/shard_map/all_gather | solution.py:59
  97.6 2.4 convolution_convert_fusion.1
  101.2 0.8 dynamic_slice.7
  102.0 19.2 %reduce-scatter.3.cloned.1.call-done = bf16[128,512]{1,0:T(8,128)(2,1)} async-done(((bf16[128,2048]{1,0:T(8,128)(2,1)}), bf16[128,512]{1,0:T(8,128)(2,1)}) %reduce-scatter.3.cloned.1.call-update) | async-done | bytes 131088 | tf_op jit(solution)/shard_map/reduce_scatter | solution.py:84
  121.2 1.0 fusion.15
  122.2 5.8 %all-reduce.1 = (f32[128]{0:T(128)S(1)}, f32[128]{0:T(128)S(1)}) all-reduce(f32[128]{0:T(128)S(1)} %get-tuple-element.6, f32[128]{0:T(128)S(1)} %get-tuple-element.5), channel_id=1, replica_groups=mesh['grp'=2,'fs'=4,'tp'=4] {'tp'}, use_global_device_ids=true, to_apply=%region_10.11 | all-reduce | flops 256 | bytes 2048 | tf_op jit(solution)/shard_map/psum | solution.py:90
  128.0 1.0 multiply_convert_fusion.1
  129.0 6.9 %all_gather.21 = bf16[128,2048]{1,0:T(8,128)(2,1)S(1)} all-gather(bf16[128,512]{1,0:T(8,128)(2,1)S(1)} %multiply_convert_fusion.1), channel_id=1, replica_groups=mesh['grp'=2,'fs'=4,'tp'=4] {'tp'}, dimensions={1}, use_global_device_ids=true | all-gather | bytes 655360 | tf_op jit(solution)/shard_map/all_gather | solution.py:92
  135.9 136.3 %all-gather.12.cloned.1.call-done = bf16[2048,2048]{1,0:T(8,128)(2,1)} async-done(((bf16[512,2048]{1,0:T(8,128)(2,1)}), bf16[2048,2048]{1,0:T(8,128)(2,1)}) %all-gather.12.cloned.1.call-update) | async-done | bytes 8388624 | tf_op jit(solution)/shard_map/all_gather | solution.py:60
  272.2 149.3 %all-gather.14.cloned.1.call-done = bf16[2048,2048]{0,1:T(8,128)(2,1)} async-done(((bf16[512,2048]{0,1:T(8,128)(2,1)}), bf16[2048,2048]{0,1:T(8,128)(2,1)}) %all-gather.14.cloned.1.call-update) | async-done | bytes 8388624 | tf_op jit(solution)/shard_map/all_gather | solution.py:61
  421.5 8.9 %convolution_convert_fusion = bf16[128,2048]{1,0:T(8,128)(2,1)} fusion(bf16[2048,2048]{0,1:T(8,128)(2,1)} %all-gather.14.cloned.1.call-done, bf16[128,2048]{1,0:T(8,128)(2,1)S(1)} %all_gather.21, bf16[2048,2048]{1,0:T(8,128)(2,1)} %all-gather.12.cloned.1.call-done), kind=kOutput, calls=%fused_computation.2 | convolution fusion | flops 2148532224 | bytes 17825792 | tf_op jit(solution)/shard_map/dot_general | solution.py:30
  430.5 20.0 %reduce-scatter.5.cloned.1.call-done = bf16[128,512]{1,0:T(8,128)(2,1)} async-done(((bf16[128,2048]{1,0:T(8,128)(2,1)}), bf16[128,512]{1,0:T(8,128)(2,1)}) %reduce-scatter.5.cloned.1.call-update) | async-done | bytes 131088 | tf_op jit(solution)/shard_map/reduce_scatter | solution.py:97
  450.4 1.0 fusion.16
  451.5 5.8 %all-reduce = (f32[128]{0:T(128)S(1)}, f32[128]{0:T(128)S(1)}) all-reduce(f32[128]{0:T(128)S(1)} %get-tuple-element.8, f32[128]{0:T(128)S(1)} %get-tuple-element.7), channel_id=1, replica_groups=mesh['grp'=2,'fs'=4,'tp'=4] {'tp'}, use_global_device_ids=true, to_apply=%region_15.16 | all-reduce | flops 256 | bytes 2048 | tf_op jit(solution)/shard_map/psum | solution.py:99
  457.2 1.7 fusion.17
  (28 shorter events, 3.6 us)
Async XLA Ops:
  6.5 63.6 %copy-start = (bf16[31,256]{1,0:T(8,128)(2,1)S(1)}, bf16[31,256]{1,0:T(8,128)(2,1)}, u32[]{:S(2)}) copy-start(bf16[31,256]{1,0:T(8,128)(2,1)} %param.16) | copy-start | bytes 47620
  6.5 91.0 %copy-start.3 = (f32[256]{0:T(256)S(1)}, f32[256]{0:T(256)}, u32[]{:S(2)}) copy-start(f32[256]{0:T(256)} %param.17) | copy-start | bytes 3076
  6.5 91.0 %copy-start.2 = (f32[256]{0:T(256)S(1)}, f32[256]{0:T(256)}, u32[]{:S(2)}) copy-start(f32[256]{0:T(256)} %param.18) | copy-start | bytes 3076
  6.5 33.1 %all-gather.6.cloned.1.call-start = ((), (), s32[]{:S(2)}) async-start(), calls=%async_computation.2 | async-start | bytes 1310720 | tf_op jit(solution)/shard_map/all_gather | solution.py:57
  7.3 61.3 %all-gather.8.cloned.1.call-start = ((), (), s32[]{:S(2)}) async-start(), calls=%async_computation.3 | async-start | bytes 1310720 | tf_op jit(solution)/shard_map/all_gather | solution.py:58
  8.0 89.6 %all-gather.10.cloned.1.call-start = ((), (), s32[]{:S(2)}) async-start(), calls=%async_computation.4 | async-start | bytes 1310720 | tf_op jit(solution)/shard_map/all_gather | solution.py:59
  8.7 112.4 %reduce-scatter.3.cloned.1.call-start = ((), (), s32[]{:S(2)}) async-start(), calls=%async_computation.5 | async-start | bytes 655360 | tf_op jit(solution)/shard_map/reduce_scatter | solution.py:84
  100.0 172.2 %all-gather.12.cloned.1.call-start = ((), (), s32[]{:S(2)}) async-start(), calls=%async_computation.6 | async-start | bytes 10485760 | tf_op jit(solution)/shard_map/all_gather | solution.py:60
  100.6 320.9 %all-gather.14.cloned.1.call-start = ((), (), s32[]{:S(2)}) async-start(), calls=%async_computation.7 | async-start | bytes 10485760 | tf_op jit(solution)/shard_map/all_gather | solution.py:61
  101.2 349.2 %reduce-scatter.5.cloned.1.call-start = ((), (), s32[]{:S(2)}) async-start(), calls=%async_computation.8 | async-start | bytes 655360 | tf_op jit(solution)/shard_map/reduce_scatter | solution.py:97
  135.9 321.3 %copy-start.1 = (f32[512]{0:T(512)S(1)}, f32[512]{0:T(512)}, u32[]{:S(2)}) copy-start(f32[512]{0:T(512)} %param.23) | copy-start | bytes 6148
Sparse Core Ops, SparseCore 0:
  8.9 30.6 all-gather.5
  41.2 27.3 all-gather.7
  70.2 27.3 all-gather.9
  100.1 20.9 reduce-scatter.2
  122.6 149.6 all-gather.11
  273.7 147.7 all-gather.13
  430.6 19.7 reduce-scatter.4
where the time goes:
time: 466 us
  waiting for transfers between devices  401 us (86%)
  blocking collectives  24.5 us (5%)
  matrix products  16.6 us (4%)
  between operations  13.5 us (3%)
  other arithmetic  8.9 us (2%)
    all_gather x1, waiting for transfers between devices, shards(): lax.all_gather(down_turned_shard, 'fs', axis=0, tiled=True)  149 us
    all_gather x1, waiting for transfers between devices, shards(): lax.all_gather(up_weight, 'fs', axis=0, tiled=True)  136 us
    all_gather x1, waiting for transfers between devices, shards(): lax.all_gather(gate_weight, 'fs', axis=0, tiled=True)  27.4 us
    all_gather x1, waiting for transfers between devices, shards(): lax.all_gather(value_weight, 'fs', axis=0, tiled=True)  26.9 us
    reduce_scatter x1, waiting for transfers between devices, shards(): lax.psum_scatter(fed_terms.astype(jnp.bfloat16), 'tp', scatter_dimension=...  20 us
    reduce_scatter x1, waiting for transfers between devices, shards(): lax.psum_scatter(partial_terms.astype(jnp.bfloat16), 'tp', scatter_dimens...  19.2 us
    all_gather x1, waiting for transfers between devices, shards(): lax.all_gather(out_turned_shard, 'fs', axis=0, tiled=True)  19 us
    dot_general x2, matrix products, contract(): lax.dot_general(left, turned, (((1,), (1,)), ((), ())), preferred_element...  11.3 us
  transfers between devices with their start and end apart: 7, of which 7 were waited for; matrix products, arithmetic and copies ran while one was open for 3% of the time, Pallas kernels for 0%

commit v1 on v0

--- a/solution.py
+++ b/solution.py
@@ -1,6 +1,10 @@
+import functools
+
 import jax
 import jax.numpy as jnp
 from jax import lax
+from jax.experimental import pallas as pl
+from jax.experimental.pallas import tpu as pltpu
 from jax.sharding import PartitionSpec as P
 
 KW = 31
@@ -101,6 +105,452 @@
     return result.reshape(seq_count, seq_length, slice_width)
 
 
+def to_rows(sums, squares):
+    lane = lax.broadcasted_iota(jnp.int32, (sums.shape[0], 128), 1)
+    spread = jnp.where(lane == 0, sums, jnp.where(lane == 1, squares, 0.0))
+    return jnp.transpose(spread)[:8]
+
+
+def from_rows(rows):
+    filler = jnp.zeros((128 - rows.shape[0], rows.shape[1]), jnp.float32)
+    columns = jnp.transpose(jnp.concatenate([rows, filler], axis=0))
+    return columns[:, 0:1], columns[:, 1:2]
+
+
+def normalize(values, sums, squares, width, gain):
+    mean = sums / width
+    var = squares / width - mean * mean
+    return (values - mean) * lax.rsqrt(var + norm_epsilon) * gain
+
+
+def layer_kernel(
+    fs_count,
+    seq_length,
+    stream,
+    in_gain,
+    value_weight,
+    gate_weight,
+    conv_kernel,
+    conv_gain,
+    conv_shift,
+    out_weight,
+    norm_gain,
+    up_hbm,
+    down_hbm,
+    out_gain,
+    out,
+    up,
+    down,
+    normed_send,
+    normed_all,
+    gate_send,
+    gate_recv,
+    padded,
+    stat_send,
+    stat_recv,
+    active_all,
+    mix_send,
+    mix_recv,
+    settled_all,
+    settled_turned,
+    up_send,
+    up_recv,
+    hidden_all,
+    fed_total,
+    fed_send,
+    fed_recv,
+    load_sem,
+    normed_ss,
+    normed_rs,
+    gate_ss,
+    gate_rs,
+    stat_ss,
+    stat_rs,
+    active_ss,
+    active_rs,
+    mix_ss,
+    mix_rs,
+    settled_ss,
+    settled_rs,
+    turned_ss,
+    turned_rs,
+    up_ss,
+    up_rs,
+    hidden_ss,
+    hidden_rs,
+    fed_ss,
+    fed_rs,
+):
+    n = fs_count
+    f = lax.axis_index("fs")
+    t = lax.axis_index("tp")
+    rows, width = stream.shape
+    own_width = width // n
+    channels = value_weight.shape[1]
+    chunks, _, chunk = up_send.shape[1:]
+    bf16, f32 = jnp.bfloat16, jnp.float32
+
+    def remote(src, dst, ss, rs, fs, tp):
+        return pltpu.make_async_remote_copy(
+            src_ref=src,
+            dst_ref=dst,
+            send_sem=ss,
+            recv_sem=rs,
+            device_id={"fs": fs, "tp": tp},
+            device_id_type=pl.DeviceIdType.MESH,
+        )
+
+    def dot(left, right):
+        return jnp.dot(left, right, preferred_element_type=f32)
+
+    up_load = pltpu.make_async_copy(up_hbm, up, load_sem.at[0])
+    down_load = pltpu.make_async_copy(down_hbm, down, load_sem.at[1])
+    up_load.start()
+    down_load.start()
+    barrier = pltpu.get_barrier_semaphore()
+    for a in range(n):
+        for b in range(n):
+            if a or b:
+                pl.semaphore_signal(
+                    barrier,
+                    inc=1,
+                    device_id={"fs": lax.rem(f + a, n), "tp": lax.rem(t + b, n)},
+                    device_id_type=pl.DeviceIdType.MESH,
+                )
+
+    def norm_in(i, carry):
+        at = pl.ds(pl.multiple_of(i * 16, 16), 16)
+        normed = norm_rows(stream[at, :].astype(f32), in_gain[...]).astype(bf16)
+        for a in range(n):
+            normed_send[a, at, :] = normed[:, a * own_width : (a + 1) * own_width]
+        return carry
+
+    lax.fori_loop(0, rows // 16, norm_in, 0)
+    pl.semaphore_wait(barrier, n * n - 1)
+
+    def peer(base, j):
+        return lax.rem(base + j, n)
+
+    waits = []
+    for j in range(1, n):
+        to = peer(f, j)
+        copy = remote(normed_send.at[to], normed_all.at[f], normed_ss.at[to], normed_rs.at[f], to, t)
+        copy.start()
+        waits.append(copy)
+    normed_all[f] = normed_send[f]
+
+    for j in range(1, n + 1):
+        to = peer(f, j)
+        if j < n:
+            remote(normed_send.at[to], normed_all.at[to], normed_ss.at[to], normed_rs.at[to], to, t).wait_recv()
+        values = dot(normed_all[to], value_weight[...])
+        gating = dot(normed_all[to], gate_weight[...])
+        if j < n:
+            gate_send[to, :, :channels] = values.astype(bf16)
+            gate_send[to, :, channels:] = gating.astype(bf16)
+            copy = remote(gate_send.at[to], gate_recv.at[f], gate_ss.at[to], gate_rs.at[f], to, t)
+            copy.start()
+            waits.append(copy)
+    for j in range(1, n):
+        at = peer(f, j)
+        remote(gate_send.at[at], gate_recv.at[at], gate_ss.at[at], gate_rs.at[at], at, t).wait_recv()
+        got = gate_recv[at].astype(f32)
+        values = values + got[:, :channels]
+        gating = gating + got[:, channels:]
+    gated = (values * jax.nn.sigmoid(gating)).astype(bf16).astype(f32)
+
+    taps = conv_kernel.shape[0]
+    pad = padded.shape[1] - seq_length
+    pieces = []
+    for s in range(rows // seq_length):
+        padded[s, :pad, :] = jnp.zeros((pad, channels), f32)
+        padded[s, pad:, :] = gated[s * seq_length : (s + 1) * seq_length]
+        total = jnp.zeros((seq_length, channels), f32)
+        for k in range(taps):
+            start = pad - (taps - 1) + k
+            total = total + padded[s, start : start + seq_length, :] * conv_kernel[k : k + 1, :].astype(f32)
+        pieces.append(total)
+    convolved = pieces[0] if len(pieces) == 1 else jnp.concatenate(pieces, axis=0)
+
+    def shared_sums(which, values, axis):
+        sums = jnp.sum(values, axis=1, keepdims=True)
+        squares = jnp.sum(values * values, axis=1, keepdims=True)
+        mine = to_rows(sums, squares)
+        stat_send[which] = mine
+        me = f if axis == "fs" else t
+        for j in range(1, n):
+            to = peer(me, j)
+            copy = remote(
+                stat_send.at[which],
+                stat_recv.at[which, me],
+                stat_ss.at[which, to],
+                stat_rs.at[which, me],
+                to if axis == "fs" else f,
+                to if axis == "tp" else t,
+            )
+            copy.start()
+            waits.append(copy)
+        for j in range(1, n):
+            at = peer(me, j)
+            remote(
+                stat_send.at[which],
+                stat_recv.at[which, at],
+                stat_ss.at[which, at],
+                stat_rs.at[which, at],
+                at if axis == "fs" else f,
+                at if axis == "tp" else t,
+            ).wait_recv()
+            mine = mine + stat_recv[which, at]
+        return from_rows(mine)
+
+    sums, squares = shared_sums(0, convolved, "tp")
+    activated = jax.nn.silu(
+        normalize(convolved, sums, squares, channels * n, conv_gain[...]) + conv_shift[...]
+    ).astype(bf16)
+    active_all[f] = activated
+    for j in range(1, n):
+        to = peer(f, j)
+        copy = remote(active_all.at[f], active_all.at[f], active_ss.at[to], active_rs.at[f], to, t)
+        copy.start()
+        waits.append(copy)
+
+    for j in range(1, n + 1):
+        at = peer(t, j)
+
+        @pl.when(at != f)
+        def _():
+            remote(active_all.at[at], active_all.at[at], active_ss.at[at], active_rs.at[at], at, t).wait_recv()
+
+        mix_send[at] = dot(active_all[at], out_weight[...]).astype(bf16)
+        if j < n:
+            copy = remote(mix_send.at[at], mix_recv.at[t], mix_ss.at[at], mix_rs.at[t], f, at)
+            copy.start()
+            waits.append(copy)
+    mixed = mix_send[t].astype(f32)
+    for j in range(1, n):
+        at = peer(t, j)
+        remote(mix_send.at[at], mix_recv.at[at], mix_ss.at[at], mix_rs.at[at], f, at).wait_recv()
+        mixed = mixed + mix_recv[at].astype(f32)
+    summed = residual_scale * normed_all[t].astype(f32) + mixed.astype(bf16).astype(f32)
+    sums, squares = shared_sums(1, summed, "fs")
+    gain_own = norm_gain[:, pl.ds(pl.multiple_of(f * own_width, 128), own_width)]
+    settled_all[t] = normalize(summed, sums, squares, width, gain_own).astype(bf16)
+    for j in range(1, n):
+        to = peer(t, j)
+        copy = remote(settled_all.at[t], settled_all.at[t], settled_ss.at[to], settled_rs.at[t], f, to)
+        copy.start()
+        waits.append(copy)
+    turned = remote(settled_all.at[t], settled_turned, turned_ss, turned_rs, t, f)
+
+    @pl.when(f != t)
+    def _():
+        turned.start()
+
+    @pl.when(f == t)
+    def _():
+        settled_turned[...] = settled_all[t]
+
+    up_load.wait()
+    for j in range(1, n):
+        at = peer(t, j)
+        remote(settled_all.at[at], settled_all.at[at], settled_ss.at[at], settled_rs.at[at], f, at).wait_recv()
+
+    def columns(c):
+        return pl.ds(pl.multiple_of(c * chunk, 128), chunk)
+
+    def up_step(c, carry):
+        for j in range(1, n):
+            to = peer(f, j)
+            up_send[to, c] = dot(settled_all[to], up[:, columns(c)]).astype(bf16)
+            remote(up_send.at[to, c], up_recv.at[f, c], up_ss.at[to, c], up_rs.at[f, c], to, t).start()
+        return carry
+
+    lax.fori_loop(0, chunks, up_step, 0)
+
+    def hidden_step(c, carry):
+        total = dot(settled_all[f], up[:, columns(c)])
+        for j in range(1, n):
+            at = peer(f, j)
+            remote(up_send.at[at, c], up_recv.at[at, c], up_ss.at[at, c], up_rs.at[at, c], at, t).wait()
+            total = total + up_recv[at, c].astype(f32)
+        hidden_all[f, c] = jnp.square(jnp.maximum(total, 0.0)).astype(bf16)
+        for j in range(1, n):
+            to = peer(f, j)
+            remote(
+                hidden_all.at[f, c], hidden_all.at[f, c], hidden_ss.at[to, c], hidden_rs.at[f, c], to, t
+            ).start()
+        return carry
+
+    lax.fori_loop(0, chunks, hidden_step, 0)
+    down_load.wait()
+    fed_total[...] = jnp.zeros_like(fed_total)
+
+    def down_step(c, carry):
+        part = down[pl.ds(pl.multiple_of(c * chunk, 128), chunk), :]
+        for j in range(n):
+            at = peer(f, j)
+            if j > 0:
+                remote(
+                    hidden_all.at[at, c], hidden_all.at[at, c], hidden_ss.at[at, c], hidden_rs.at[at, c], at, t
+                ).wait()
+            fed_total[at] += dot(hidden_all[at, c], part)
+        return carry
+
+    lax.fori_loop(0, chunks, down_step, 0)
+    for j in range(1, n + 1):
+        at = peer(f, j)
+        fed_send[at] = fed_total[at].astype(bf16)
+        copy = remote(fed_send.at[at], fed_recv.at[t], fed_ss.at[at], fed_rs.at[t], at, f)
+        if j < n:
+            copy.start()
+            waits.append(copy)
+        else:
+
+            @pl.when(f != t)
+            def _():
+                copy.start()
+
+            @pl.when(f == t)
+            def _():
+                fed_recv[t] = fed_send[f]
+
+    last = copy
+
+    @pl.when(f != t)
+    def _():
+        turned.wait()
+
+    fed = jnp.zeros((rows, own_width), f32)
+    for b in range(n):
+        got = remote(fed_send.at[b], fed_recv.at[b], fed_ss.at[b], fed_rs.at[b], t, b)
+
+        @pl.when(jnp.logical_not(jnp.logical_and(f == t, t == b)))
+        def _():
+            got.wait_recv()
+
+        fed = fed + fed_recv[b].astype(f32)
+    final = residual_scale * settled_turned[...].astype(f32) + fed.astype(bf16).astype(f32)
+    sums, squares = shared_sums(2, final, "tp")
+    out[...] = normalize(final, sums, squares, width, out_gain[...]).astype(bf16)
+    for copy in waits:
+        copy.wait_send()
+
+    @pl.when(f != t)
+    def _():
+        last.wait_send()
+
+
+def fast_shards(
+    stream,
+    in_gain,
+    value_weight,
+    gate_weight,
+    conv_kernel,
+    conv_gain,
+    conv_shift,
+    out_weight,
+    norm_gain,
+    up_weight,
+    down_weight,
+    out_gain,
+):
+    seq_count, seq_length, width = stream.shape
+    rows = seq_count * seq_length
+    n = lax.axis_size("fs")
+    own = width // n
+    channels = value_weight.shape[1]
+    units = up_weight.shape[1]
+    chunk = units // 4
+    chunks = units // chunk
+    taps = conv_kernel.shape[0]
+    pad = -(-(taps - 1) // 8) * 8
+    bf16, f32 = jnp.bfloat16, jnp.float32
+    vmem, dma = pltpu.VMEM, pltpu.SemaphoreType.DMA
+    whole = pl.BlockSpec(memory_space=pltpu.VMEM)
+    far = pl.BlockSpec(memory_space=pl.ANY)
+    result = pl.pallas_call(
+        functools.partial(layer_kernel, n, seq_length),
+        out_shape=jax.ShapeDtypeStruct((rows, own), bf16),
+        in_specs=[whole] * 9 + [far, far, whole],
+        out_specs=whole,
+        scratch_shapes=[
+            vmem(up_weight.shape, bf16),
+            vmem(down_weight.shape, bf16),
+            vmem((n, rows, own), bf16),
+            vmem((n, rows, own), bf16),
+            vmem((n, rows, 2 * channels), bf16),
+            vmem((n, rows, 2 * channels), bf16),
+            vmem((seq_count, pad + seq_length, channels), f32),
+            vmem((3, 8, rows), f32),
+            vmem((3, n, 8, rows), f32),
+            vmem((n, rows, channels), bf16),
+            vmem((n, rows, own), bf16),
+            vmem((n, rows, own), bf16),
+            vmem((n, rows, own), bf16),
+            vmem((rows, own), bf16),
+            vmem((n, chunks, rows, chunk), bf16),
+            vmem((n, chunks, rows, chunk), bf16),
+            vmem((n, chunks, rows, chunk), bf16),
+            vmem((n, rows, own), f32),
+            vmem((n, rows, own), bf16),
+            vmem((n, rows, own), bf16),
+            dma((2,)),
+            dma((n,)),
+            dma((n,)),
+            dma((n,)),
+            dma((n,)),
+            dma((3, n)),
+            dma((3, n)),
+            dma((n,)),
+            dma((n,)),
+            dma((n,)),
+            dma((n,)),
+            dma((n,)),
+            dma((n,)),
+            dma,
+            dma,
+            dma((n, chunks)),
+            dma((n, chunks)),
+            dma((n, chunks)),
+            dma((n, chunks)),
+            dma((n,)),
+            dma((n,)),
+        ],
+        compiler_params=pltpu.CompilerParams(
+            collective_id=0, has_side_effects=True, vmem_limit_bytes=60 * 1024 * 1024
+        ),
+    )(
+        stream.reshape(rows, width),
+        in_gain[None],
+        value_weight,
+        gate_weight,
+        conv_kernel,
+        conv_gain[None],
+        conv_shift[None],
+        out_weight,
+        norm_gain[None],
+        up_weight,
+        down_weight,
+        out_gain[None],
+    )
+    return result.reshape(seq_count, seq_length, own)
+
+
+def layer(*args):
+    stream, value_weight, up_weight = args[0], args[2], args[9]
+    n = lax.axis_size("fs")
+    fits = (
+        n == lax.axis_size("tp")
+        and n > 1
+        and stream.shape[0] * stream.shape[1] == 128
+        and stream.shape[1] % 8 == 0
+        and stream.shape[2] % (128 * n) == 0
+        and value_weight.shape[1] % 128 == 0
+        and up_weight.shape[1] % 512 == 0
+    )
+    return fast_shards(*args) if fits else shards(*args)
+
+
 def solution(mesh):
     in_specs = (
         P(("grp", "fs"), None, None),
@@ -117,4 +567,4 @@
         P("tp"),
     )
     out_specs = P(("grp", "fs"), None, "tp")
-    return jax.shard_map(shards, mesh=mesh, in_specs=in_specs, out_specs=out_specs, check_vma=False)
+    return jax.shard_map(layer, mesh=mesh, in_specs=in_specs, out_specs=out_specs, check_vma=False)

time: 466 us -> 168 us (0.36)
  waiting for transfers between devices: 401 us -> 0 us
  Pallas kernels: 0 us -> 166 us
  blocking collectives: 24.5 us -> 0 us
  matrix products: 16.6 us -> 0 us
  between operations: 13.5 us -> 0.01 us
  other arithmetic: 8.9 us -> 0 us
    all_gather x5 -> x0, waiting for transfers between devices: 359 us -> none  [the longest x1 149 us: shards(): lax.all_gather(down_turned_shard, 'fs', axis=0, tiled=True)]
    pallas_call x0 -> x1, Pallas kernels: none -> 166 us  [fast_shards(): pl.pallas_call(functools.partial(layer_kernel, n, seq_length), out_shape=...]
    reduce_scatter x2 -> x0, waiting for transfers between devices: 39.1 us -> none  [the longest x1 20 us: shards(): lax.psum_scatter(fed_terms.astype(jnp.bfloat16), 'tp', scatter_dimension=...]
    psum x3 -> x0, blocking collectives: 17.6 us -> none  [the longest x1 6.08 us: shards(): conv_sums = lax.psum(row_sums(convolved), 'tp')]
    dot_general x4 -> x0, matrix products: 14.4 us -> none  [the longest x2 11.3 us: contract(): lax.dot_general(left, turned, (((1,), (1,)), ((), ())), preferred_element...]
    all_gather x1 -> x0, blocking collectives: 6.86 us -> none  [shards(): settled_full = lax.all_gather(settled_own, 'tp', axis=1, tiled=True)]
    reduce_sum x5 -> x0, other arithmetic: 4.72 us -> none  [the longest x3 2.2 us: row_sums(): return (jnp.sum(summed, axis=1), jnp.sum(summed * summed, axis=1))]
  transfers between devices with their start and end apart: 7 -> 0, of which waited for: 7 -> 0; matrix products, arithmetic and copies ran while one was open for 3% -> 0% of each run, Pallas kernels for 0% -> 0%
where the time goes in v1:
time: 168 us; the launch traced here: 167 us
  Pallas kernels  166 us (99%)
    pallas_call x1, Pallas kernels, fast_shards(): pl.pallas_call(functools.partial(layer_kernel, n, seq_length), out_shape=...  166 us

profile of v1, /device:TPU:0, one launch (start us, length us, event | category | flops | bytes accessed | tf_op | source)
XLA Modules:
  0.0 167.4 jit_solution(5786753831974009030)
XLA Ops:
  0.0 165.8 %shard_map.118 = bf16[128,512]{1,0:T(8,128)(2,1)} custom-call(bf16[128,2048]{1,0:T(8,128)(2,1)} %bitcast.7, f32[1,2048]{1,0:T(1,128)} %bitcast.9, bf16[512,256]{1,0:T(8,128)(2,1)} %value_weight.1, bf16[512,256]{1,0:T(8,128)(2,1)} %gate_weight.1, bf16[31,256]{1,0:T(8,128)(2,1)} %conv_kernel.1, f32[1,256]{1,0:T(1,128)} %bitcast.12, f32[1,256]{1,0:T(1,128)} %bitcast.13, ...), custom_call_target="tpu_custom_call" | custom-call | tf_op jit(solution)/shard_map/pallas_call | solution.py:471
  165.8 1.6 copy.14

commit v2 on v1

--- a/solution.py
+++ b/solution.py
@@ -8,6 +8,7 @@
 from jax.sharding import PartitionSpec as P
 
 KW = 31
+UP_A, UP_B, DN_A, DN_B = (1, 2), (3,), (1, 2), (3,)
 
 
 norm_epsilon = 1e-05
@@ -152,14 +153,19 @@
     mix_send,
     mix_recv,
     settled_all,
-    settled_turned,
-    up_send,
-    up_recv,
-    hidden_all,
-    fed_total,
+    hidden,
+    pair_own,
+    pair_send,
+    pair_recv,
+    cross_send,
+    cross_recv,
     fed_send,
     fed_recv,
     load_sem,
+    up_ss,
+    up_rs,
+    down_ss,
+    down_rs,
     normed_ss,
     normed_rs,
     gate_ss,
@@ -172,41 +178,49 @@
     mix_rs,
     settled_ss,
     settled_rs,
-    turned_ss,
-    turned_rs,
-    up_ss,
-    up_rs,
-    hidden_ss,
-    hidden_rs,
+    pair_ss,
+    pair_rs,
+    cross_ss,
+    cross_rs,
     fed_ss,
     fed_rs,
 ):
     n = fs_count
     f = lax.axis_index("fs")
     t = lax.axis_index("tp")
+    g = lax.axis_index("grp")
+    side = lax.rem(t, 2)
+    mate = t + 1 - 2 * side
+    across = lax.rem(t + 2, n)
     rows, width = stream.shape
     own_width = width // n
     channels = value_weight.shape[1]
-    chunks, _, chunk = up_send.shape[1:]
+    half_units = up.shape[3]
+    units = 2 * half_units
     bf16, f32 = jnp.bfloat16, jnp.float32
 
-    def remote(src, dst, ss, rs, fs, tp):
+    def remote(src, dst, ss, rs, fs, tp, grp=g):
         return pltpu.make_async_remote_copy(
             src_ref=src,
             dst_ref=dst,
             send_sem=ss,
             recv_sem=rs,
-            device_id={"fs": fs, "tp": tp},
+            device_id={"grp": grp, "fs": fs, "tp": tp},
             device_id_type=pl.DeviceIdType.MESH,
         )
 
     def dot(left, right):
         return jnp.dot(left, right, preferred_element_type=f32)
 
-    up_load = pltpu.make_async_copy(up_hbm, up, load_sem.at[0])
-    down_load = pltpu.make_async_copy(down_hbm, down, load_sem.at[1])
-    up_load.start()
-    down_load.start()
+    def share(block, h):
+        return pl.ds(pl.multiple_of(block * units + h * half_units, 128), half_units)
+
+    loads = []
+    for h in range(2):
+        loads.append(pltpu.make_async_copy(up_hbm.at[:, share(f, h)], up.at[h, f], load_sem.at[0, h]))
+        loads.append(pltpu.make_async_copy(down_hbm.at[share(f, h), :], down.at[h, f], load_sem.at[1, h]))
+    for load in loads:
+        load.start()
     barrier = pltpu.get_barrier_semaphore()
     for a in range(n):
         for b in range(n):
@@ -218,6 +232,13 @@
                     device_id_type=pl.DeviceIdType.MESH,
                 )
 
+    pl.semaphore_signal(
+        barrier,
+        inc=1,
+        device_id={"grp": 1 - g, "fs": f, "tp": t},
+        device_id_type=pl.DeviceIdType.MESH,
+    )
+
     def norm_in(i, carry):
         at = pl.ds(pl.multiple_of(i * 16, 16), 16)
         normed = norm_rows(stream[at, :].astype(f32), in_gain[...]).astype(bf16)
@@ -226,23 +247,64 @@
         return carry
 
     lax.fori_loop(0, rows // 16, norm_in, 0)
-    pl.semaphore_wait(barrier, n * n - 1)
-
     def peer(base, j):
         return lax.rem(base + j, n)
 
     waits = []
-    for j in range(1, n):
-        to = peer(f, j)
-        copy = remote(normed_send.at[to], normed_all.at[f], normed_ss.at[to], normed_rs.at[f], to, t)
+
+    def up_copy(to, at):
+        return remote(up_hbm.at[:, share(to, g)], up.at[g, at], up_ss.at[0, to], up_rs.at[0, at], to, t)
+
+    def down_copy(to, at):
+        return remote(down_hbm.at[share(to, g), :], down.at[g, at], down_ss.at[0, to], down_rs.at[0, at], to, t)
+
+    def start(copy):
         copy.start()
         waits.append(copy)
+
+    def send_weights(make, steps):
+        for j in steps:
+            start(make(peer(f, j), f))
+
+    def swap_weights(make, held, ss, rs):
+        for j in range(1, n):
+            at = peer(f, n - j)
+            make(at, at).wait_recv()
+            start(remote(held.at[g, at], held.at[g, at], ss.at[1, at], rs.at[1, at], f, t, 1 - g))
+
+    def swap_wait(held, ss, rs):
+        for j in range(1, n):
+            at = peer(f, n - j)
+            remote(held.at[1 - g, at], held.at[1 - g, at], ss.at[1, at], rs.at[1, at], f, t, 1 - g).wait_recv()
+
+    half = rows // 2
+    mine = pl.ds(pl.multiple_of(side * half, half), half)
+    theirs = pl.ds(pl.multiple_of((1 - side) * half, half), half)
+
+    def normed_copy(to, at):
+        return remote(
+            normed_send.at[to, mine], normed_all.at[at, mine], normed_ss.at[0, to], normed_rs.at[0, at], to, t
+        )
+
+    def normed_pass(at, part):
+        return remote(
+            normed_all.at[at, part], normed_all.at[at, part], normed_ss.at[1, at], normed_rs.at[1, at], f, mate
+        )
+
+    pl.semaphore_wait(barrier, n * n)
+    for j in range(1, n):
+        start(normed_copy(peer(f, j), f))
+    send_weights(up_copy, UP_A)
     normed_all[f] = normed_send[f]
+    for j in range(1, n):
+        at = peer(f, j)
+        normed_copy(at, at).wait_recv()
+        start(normed_pass(at, mine))
 
     for j in range(1, n + 1):
         to = peer(f, j)
         if j < n:
-            remote(normed_send.at[to], normed_all.at[to], normed_ss.at[to], normed_rs.at[to], to, t).wait_recv()
+            normed_pass(to, theirs).wait_recv()
         values = dot(normed_all[to], value_weight[...])
         gating = dot(normed_all[to], gate_weight[...])
         if j < n:
@@ -251,6 +313,7 @@
             copy = remote(gate_send.at[to], gate_recv.at[f], gate_ss.at[to], gate_rs.at[f], to, t)
             copy.start()
             waits.append(copy)
+    send_weights(up_copy, UP_B)
     for j in range(1, n):
         at = peer(f, j)
         remote(gate_send.at[at], gate_recv.at[at], gate_ss.at[at], gate_rs.at[at], at, t).wait_recv()
@@ -267,12 +330,12 @@
         padded[s, pad:, :] = gated[s * seq_length : (s + 1) * seq_length]
         total = jnp.zeros((seq_length, channels), f32)
         for k in range(taps):
-            start = pad - (taps - 1) + k
-            total = total + padded[s, start : start + seq_length, :] * conv_kernel[k : k + 1, :].astype(f32)
+            begin = pad - (taps - 1) + k
+            total = total + padded[s, begin : begin + seq_length, :] * conv_kernel[k : k + 1, :].astype(f32)
         pieces.append(total)
     convolved = pieces[0] if len(pieces) == 1 else jnp.concatenate(pieces, axis=0)
 
-    def shared_sums(which, values, axis):
+    def shared_sums(which, values, axis, then=()):
         sums = jnp.sum(values, axis=1, keepdims=True)
         squares = jnp.sum(values * values, axis=1, keepdims=True)
         mine = to_rows(sums, squares)
@@ -290,6 +353,7 @@
             )
             copy.start()
             waits.append(copy)
+        send_weights(down_copy, then)
         for j in range(1, n):
             at = peer(me, j)
             remote(
@@ -310,9 +374,9 @@
     active_all[f] = activated
     for j in range(1, n):
         to = peer(f, j)
-        copy = remote(active_all.at[f], active_all.at[f], active_ss.at[to], active_rs.at[f], to, t)
-        copy.start()
-        waits.append(copy)
+        start(remote(active_all.at[f], active_all.at[f], active_ss.at[to], active_rs.at[f], to, t))
+    send_weights(down_copy, DN_A)
+    swap_weights(up_copy, up, up_ss, up_rs)
 
     for j in range(1, n + 1):
         at = peer(t, j)
@@ -332,112 +396,88 @@
         remote(mix_send.at[at], mix_recv.at[at], mix_ss.at[at], mix_rs.at[at], f, at).wait_recv()
         mixed = mixed + mix_recv[at].astype(f32)
     summed = residual_scale * normed_all[t].astype(f32) + mixed.astype(bf16).astype(f32)
-    sums, squares = shared_sums(1, summed, "fs")
+    sums, squares = shared_sums(1, summed, "fs", DN_B)
     gain_own = norm_gain[:, pl.ds(pl.multiple_of(f * own_width, 128), own_width)]
-    settled_all[t] = normalize(summed, sums, squares, width, gain_own).astype(bf16)
+    settled_all[t, f] = normalize(summed, sums, squares, width, gain_own).astype(bf16)
+
+    def settled_copy(step, group, block, fs, tp, key=None):
+        where = settled_all.at[group, block]
+        send = block if key is None else key
+        return remote(where, where, settled_ss.at[step, send], settled_rs.at[step, block], fs, tp)
+
     for j in range(1, n):
-        to = peer(t, j)
-        copy = remote(settled_all.at[t], settled_all.at[t], settled_ss.at[to], settled_rs.at[t], f, to)
-        copy.start()
-        waits.append(copy)
-    turned = remote(settled_all.at[t], settled_turned, turned_ss, turned_rs, t, f)
-
-    @pl.when(f != t)
-    def _():
-        turned.start()
-
-    @pl.when(f == t)
-    def _():
-        settled_turned[...] = settled_all[t]
-
-    up_load.wait()
+        start(settled_copy(0, t, f, peer(f, j), t, peer(f, j)))
+    for j in range(n):
+        at = peer(f, j)
+        if j > 0:
+            settled_copy(0, t, at, at, t).wait_recv()
+        start(settled_copy(1, t, at, f, across))
+        start(settled_copy(2, t, at, f, mate))
+    for j in range(n):
+        at = peer(f, j)
+        settled_copy(1, across, at, f, across).wait_recv()
+        start(settled_copy(3, across, at, f, mate))
+    swap_weights(down_copy, down, down_ss, down_rs)
+    for load in loads:
+        load.wait()
+    swap_wait(up, up_ss, up_rs)
+
+    def make_hidden(group):
+        for h in range(2):
+            total = jnp.zeros((rows, half_units), f32)
+            for b in range(n):
+                total = total + dot(settled_all[group, b], up[h, b])
+            hidden[group, h] = jnp.square(jnp.maximum(total, 0.0)).astype(bf16)
+
+    make_hidden(t)
+    for j in range(n):
+        at = peer(f, j)
+        settled_copy(2, mate, at, f, mate).wait_recv()
+    make_hidden(mate)
+    make_hidden(across)
+    opposite = lax.rem(mate + 2, n)
+    for j in range(n):
+        at = peer(f, j)
+        settled_copy(3, opposite, at, f, mate).wait_recv()
+    make_hidden(opposite)
+    swap_wait(down, down_ss, down_rs)
+
+    def fed_part(group, block):
+        return dot(hidden[group, 0], down[0, block]) + dot(hidden[group, 1], down[1, block])
+
+    def pair_copy(r):
+        return remote(pair_send.at[r], pair_recv.at[r], pair_ss.at[r], pair_rs.at[r], f, mate)
+
+    def cross_copy(r):
+        return remote(cross_send.at[r], cross_recv.at[r], cross_ss.at[r], cross_rs.at[r], f, across)
+
+    for j in range(1, n + 1):
+        r = peer(f, j)
+        pair_send[r, 0] = fed_part(r, mate).astype(bf16)
+        pair_send[r, 1] = fed_part(r, opposite).astype(bf16)
+        start(pair_copy(r))
+        pair_own[r, 0] = fed_part(r, t)
+        pair_own[r, 1] = fed_part(r, across)
+        pair_copy(r).wait_recv()
+        pair_own[r, 0] += pair_recv[r, 0].astype(f32)
+        cross_send[r] = (pair_own[r, 1] + pair_recv[r, 1].astype(f32)).astype(bf16)
+        start(cross_copy(r))
+    for j in range(1, n + 1):
+        r = peer(f, j)
+        cross_copy(r).wait_recv()
+        fed = pair_own[r, 0] + cross_recv[r].astype(f32)
+        if j < n:
+            fed_send[r] = fed.astype(bf16)
+            start(remote(fed_send.at[r], fed_recv.at[f], fed_ss.at[r], fed_rs.at[f], r, t))
     for j in range(1, n):
-        at = peer(t, j)
-        remote(settled_all.at[at], settled_all.at[at], settled_ss.at[at], settled_rs.at[at], f, at).wait_recv()
-
-    def columns(c):
-        return pl.ds(pl.multiple_of(c * chunk, 128), chunk)
-
-    def up_step(c, carry):
-        for j in range(1, n):
-            to = peer(f, j)
-            up_send[to, c] = dot(settled_all[to], up[:, columns(c)]).astype(bf16)
-            remote(up_send.at[to, c], up_recv.at[f, c], up_ss.at[to, c], up_rs.at[f, c], to, t).start()
-        return carry
-
-    lax.fori_loop(0, chunks, up_step, 0)
-
-    def hidden_step(c, carry):
-        total = dot(settled_all[f], up[:, columns(c)])
-        for j in range(1, n):
-            at = peer(f, j)
-            remote(up_send.at[at, c], up_recv.at[at, c], up_ss.at[at, c], up_rs.at[at, c], at, t).wait()
-            total = total + up_recv[at, c].astype(f32)
-        hidden_all[f, c] = jnp.square(jnp.maximum(total, 0.0)).astype(bf16)
-        for j in range(1, n):
-            to = peer(f, j)
-            remote(
-                hidden_all.at[f, c], hidden_all.at[f, c], hidden_ss.at[to, c], hidden_rs.at[f, c], to, t
-            ).start()
-        return carry
-
-    lax.fori_loop(0, chunks, hidden_step, 0)
-    down_load.wait()
-    fed_total[...] = jnp.zeros_like(fed_total)
-
-    def down_step(c, carry):
-        part = down[pl.ds(pl.multiple_of(c * chunk, 128), chunk), :]
-        for j in range(n):
-            at = peer(f, j)
-            if j > 0:
-                remote(
-                    hidden_all.at[at, c], hidden_all.at[at, c], hidden_ss.at[at, c], hidden_rs.at[at, c], at, t
-                ).wait()
-            fed_total[at] += dot(hidden_all[at, c], part)
-        return carry
-
-    lax.fori_loop(0, chunks, down_step, 0)
-    for j in range(1, n + 1):
         at = peer(f, j)
-        fed_send[at] = fed_total[at].astype(bf16)
-        copy = remote(fed_send.at[at], fed_recv.at[t], fed_ss.at[at], fed_rs.at[t], at, f)
-        if j < n:
-            copy.start()
-            waits.append(copy)
-        else:
-
-            @pl.when(f != t)
-            def _():
-                copy.start()
-
-            @pl.when(f == t)
-            def _():
-                fed_recv[t] = fed_send[f]
-
-    last = copy
-
-    @pl.when(f != t)
-    def _():
-        turned.wait()
-
-    fed = jnp.zeros((rows, own_width), f32)
-    for b in range(n):
-        got = remote(fed_send.at[b], fed_recv.at[b], fed_ss.at[b], fed_rs.at[b], t, b)
-
-        @pl.when(jnp.logical_not(jnp.logical_and(f == t, t == b)))
-        def _():
-            got.wait_recv()
-
-        fed = fed + fed_recv[b].astype(f32)
-    final = residual_scale * settled_turned[...].astype(f32) + fed.astype(bf16).astype(f32)
+        remote(fed_send.at[at], fed_recv.at[at], fed_ss.at[at], fed_rs.at[at], at, t).wait_recv()
+        fed = fed + fed_recv[at].astype(f32)
+    final = residual_scale * settled_all[f, t].astype(f32) + fed.astype(bf16).astype(f32)
     sums, squares = shared_sums(2, final, "tp")
     out[...] = normalize(final, sums, squares, width, out_gain[...]).astype(bf16)
     for copy in waits:
         copy.wait_send()
-
-    @pl.when(f != t)
-    def _():
-        last.wait_send()
 
 
 def fast_shards(
@@ -460,8 +500,7 @@
     own = width // n
     channels = value_weight.shape[1]
     units = up_weight.shape[1]
-    chunk = units // 4
-    chunks = units // chunk
+    half_units = units // n // 2
     taps = conv_kernel.shape[0]
     pad = -(-(taps - 1) // 8) * 8
     bf16, f32 = jnp.bfloat16, jnp.float32
@@ -474,8 +513,8 @@
         in_specs=[whole] * 9 + [far, far, whole],
         out_specs=whole,
         scratch_shapes=[
-            vmem(up_weight.shape, bf16),
-            vmem(down_weight.shape, bf16),
+            vmem((2, n, own, half_units), bf16),
+            vmem((2, n, half_units, own), bf16),
             vmem((n, rows, own), bf16),
             vmem((n, rows, own), bf16),
             vmem((n, rows, 2 * channels), bf16),
@@ -486,17 +525,22 @@
             vmem((n, rows, channels), bf16),
             vmem((n, rows, own), bf16),
             vmem((n, rows, own), bf16),
-            vmem((n, rows, own), bf16),
-            vmem((rows, own), bf16),
-            vmem((n, chunks, rows, chunk), bf16),
-            vmem((n, chunks, rows, chunk), bf16),
-            vmem((n, chunks, rows, chunk), bf16),
-            vmem((n, rows, own), f32),
-            vmem((n, rows, own), bf16),
-            vmem((n, rows, own), bf16),
-            dma((2,)),
-            dma((n,)),
-            dma((n,)),
+            vmem((n, n, rows, own), bf16),
+            vmem((n, 2, rows, half_units), bf16),
+            vmem((n, 2, rows, own), f32),
+            vmem((n, 2, rows, own), bf16),
+            vmem((n, 2, rows, own), bf16),
+            vmem((n, rows, own), bf16),
+            vmem((n, rows, own), bf16),
+            vmem((n, rows, own), bf16),
+            vmem((n, rows, own), bf16),
+            dma((2, 2)),
+            dma((2, n)),
+            dma((2, n)),
+            dma((2, n)),
+            dma((2, n)),
+            dma((2, n)),
+            dma((2, n)),
             dma((n,)),
             dma((n,)),
             dma((3, n)),
@@ -505,14 +549,12 @@
             dma((n,)),
             dma((n,)),
             dma((n,)),
-            dma((n,)),
-            dma((n,)),
-            dma,
-            dma,
-            dma((n, chunks)),
-            dma((n, chunks)),
-            dma((n, chunks)),
-            dma((n, chunks)),
+            dma((4, n)),
+            dma((4, n)),
+            dma((n,)),
+            dma((n,)),
+            dma((n,)),
+            dma((n,)),
             dma((n,)),
             dma((n,)),
         ],
@@ -541,12 +583,13 @@
     n = lax.axis_size("fs")
     fits = (
         n == lax.axis_size("tp")
-        and n > 1
+        and n == 4
+        and lax.axis_size("grp") == 2
         and stream.shape[0] * stream.shape[1] == 128
         and stream.shape[1] % 8 == 0
         and stream.shape[2] % (128 * n) == 0
         and value_weight.shape[1] % 128 == 0
-        and up_weight.shape[1] % 512 == 0
+        and up_weight.shape[1] % (256 * n) == 0
     )
     return fast_shards(*args) if fits else shards(*args)
 

time: 168 us -> 145 us (0.86)
  Pallas kernels: 166 us -> 143 us
    pallas_call x1, Pallas kernels: 166 us -> 143 us  [fast_shards(): pl.pallas_call(functools.partial(layer_kernel, n, seq_length), out_shape=...]
where the time goes in v2:
time: 145 us
  Pallas kernels  143 us (99%)
  local copies, waits for them, and re-layouts  1.57 us (1%)
    pallas_call x1, Pallas kernels, fast_shards(): pl.pallas_call(functools.partial(layer_kernel, n, seq_length), out_shape=...  143 us

profile of v2, /device:TPU:0, one launch (start us, length us, event | category | flops | bytes accessed | tf_op | source)
XLA Modules:
  0.0 145.0 jit_solution(10151397737444560269)
XLA Ops:
  0.0 143.4 %shard_map.118 = bf16[128,512]{1,0:T(8,128)(2,1)} custom-call(bf16[128,2048]{1,0:T(8,128)(2,1)} %bitcast.7, f32[1,2048]{1,0:T(1,128)} %bitcast.9, bf16[512,256]{1,0:T(8,128)(2,1)} %value_weight.1, bf16[512,256]{1,0:T(8,128)(2,1)} %gate_weight.1, bf16[31,256]{1,0:T(8,128)(2,1)} %conv_kernel.1, f32[1,256]{1,0:T(1,128)} %bitcast.12, f32[1,256]{1,0:T(1,128)} %bitcast.13, ...), custom_call_target="tpu_custom_call" | custom-call | tf_op jit(solution)/shard_map/pallas_call | solution.py:510
  143.4 1.6 %copy.14 = bf16[1,128,512]{2,1,0:T(8,128)(2,1)} copy(bf16[1,128,512]{2,1,0:T(8,128)(2,1)} %bitcast.8) | data formatting | bytes 262144

commit v3 on v2

--- a/solution.py
+++ b/solution.py
@@ -8,7 +8,7 @@
 from jax.sharding import PartitionSpec as P
 
 KW = 31
-UP_A, UP_B, DN_A, DN_B = (1, 2), (3,), (1, 2), (3,)
+PLAN = ("u1u2u3", "d2", "", "U1U2U3", "d1d3", "D2", "", "D1D3", "", "", "")
 
 
 norm_epsilon = 1e-05
@@ -239,6 +239,55 @@
         device_id_type=pl.DeviceIdType.MESH,
     )
 
+    def peer(base, j):
+        return lax.rem(base + j, n)
+
+    waits = []
+
+    def up_copy(to, at):
+        return remote(up_hbm.at[:, share(to, g)], up.at[g, at], up_ss.at[0, to], up_rs.at[0, at], to, t)
+
+    def down_copy(to, at):
+        return remote(down_hbm.at[share(to, g), :], down.at[g, at], down_ss.at[0, to], down_rs.at[0, at], to, t)
+
+    def start(copy):
+        copy.start()
+        waits.append(copy)
+
+    weights = {"u": (up_copy, up, up_ss, up_rs), "d": (down_copy, down, down_ss, down_rs)}
+
+    def stage(index):
+        for kind, step in zip(PLAN[index][::2], PLAN[index][1::2]):
+            make, held, ss, rs = weights[kind.lower()]
+            if kind.islower():
+                start(make(peer(f, int(step)), f))
+            else:
+                at = peer(f, n - int(step))
+                make(at, at).wait_recv()
+                start(remote(held.at[g, at], held.at[g, at], ss.at[1, at], rs.at[1, at], f, t, 1 - g))
+
+    def swap_wait(held, ss, rs):
+        for j in range(1, n):
+            at = peer(f, n - j)
+            remote(held.at[1 - g, at], held.at[1 - g, at], ss.at[1, at], rs.at[1, at], f, t, 1 - g).wait_recv()
+
+    half = rows // 2
+    mine = pl.ds(pl.multiple_of(side * half, half), half)
+    theirs = pl.ds(pl.multiple_of((1 - side) * half, half), half)
+
+    def normed_copy(to, at):
+        return remote(
+            normed_send.at[to, mine], normed_all.at[at, mine], normed_ss.at[0, to], normed_rs.at[0, at], to, t
+        )
+
+    def normed_pass(at, part):
+        return remote(
+            normed_all.at[at, part], normed_all.at[at, part], normed_ss.at[1, at], normed_rs.at[1, at], f, mate
+        )
+
+    pl.semaphore_wait(barrier, n * n)
+    stage(0)
+
     def norm_in(i, carry):
         at = pl.ds(pl.multiple_of(i * 16, 16), 16)
         normed = norm_rows(stream[at, :].astype(f32), in_gain[...]).astype(bf16)
@@ -247,54 +296,10 @@
         return carry
 
     lax.fori_loop(0, rows // 16, norm_in, 0)
-    def peer(base, j):
-        return lax.rem(base + j, n)
-
-    waits = []
-
-    def up_copy(to, at):
-        return remote(up_hbm.at[:, share(to, g)], up.at[g, at], up_ss.at[0, to], up_rs.at[0, at], to, t)
-
-    def down_copy(to, at):
-        return remote(down_hbm.at[share(to, g), :], down.at[g, at], down_ss.at[0, to], down_rs.at[0, at], to, t)
-
-    def start(copy):
-        copy.start()
-        waits.append(copy)
-
-    def send_weights(make, steps):
-        for j in steps:
-            start(make(peer(f, j), f))
-
-    def swap_weights(make, held, ss, rs):
-        for j in range(1, n):
-            at = peer(f, n - j)
-            make(at, at).wait_recv()
-            start(remote(held.at[g, at], held.at[g, at], ss.at[1, at], rs.at[1, at], f, t, 1 - g))
-
-    def swap_wait(held, ss, rs):
-        for j in range(1, n):
-            at = peer(f, n - j)
-            remote(held.at[1 - g, at], held.at[1 - g, at], ss.at[1, at], rs.at[1, at], f, t, 1 - g).wait_recv()
-
-    half = rows // 2
-    mine = pl.ds(pl.multiple_of(side * half, half), half)
-    theirs = pl.ds(pl.multiple_of((1 - side) * half, half), half)
-
-    def normed_copy(to, at):
-        return remote(
-            normed_send.at[to, mine], normed_all.at[at, mine], normed_ss.at[0, to], normed_rs.at[0, at], to, t
-        )
-
-    def normed_pass(at, part):
-        return remote(
-            normed_all.at[at, part], normed_all.at[at, part], normed_ss.at[1, at], normed_rs.at[1, at], f, mate
-        )
-
-    pl.semaphore_wait(barrier, n * n)
+
     for j in range(1, n):
         start(normed_copy(peer(f, j), f))
-    send_weights(up_copy, UP_A)
+    stage(1)
     normed_all[f] = normed_send[f]
     for j in range(1, n):
         at = peer(f, j)
@@ -313,7 +318,7 @@
             copy = remote(gate_send.at[to], gate_recv.at[f], gate_ss.at[to], gate_rs.at[f], to, t)
             copy.start()
             waits.append(copy)
-    send_weights(up_copy, UP_B)
+    stage(2)
     for j in range(1, n):
         at = peer(f, j)
         remote(gate_send.at[at], gate_recv.at[at], gate_ss.at[at], gate_rs.at[at], at, t).wait_recv()
@@ -335,7 +340,7 @@
         pieces.append(total)
     convolved = pieces[0] if len(pieces) == 1 else jnp.concatenate(pieces, axis=0)
 
-    def shared_sums(which, values, axis, then=()):
+    def shared_sums(which, values, axis, then=None):
         sums = jnp.sum(values, axis=1, keepdims=True)
         squares = jnp.sum(values * values, axis=1, keepdims=True)
         mine = to_rows(sums, squares)
@@ -353,7 +358,8 @@
             )
             copy.start()
             waits.append(copy)
-        send_weights(down_copy, then)
+        if then is not None:
+            stage(then)
         for j in range(1, n):
             at = peer(me, j)
             remote(
@@ -367,7 +373,7 @@
             mine = mine + stat_recv[which, at]
         return from_rows(mine)
 
-    sums, squares = shared_sums(0, convolved, "tp")
+    sums, squares = shared_sums(0, convolved, "tp", 3)
     activated = jax.nn.silu(
         normalize(convolved, sums, squares, channels * n, conv_gain[...]) + conv_shift[...]
     ).astype(bf16)
@@ -375,8 +381,7 @@
     for j in range(1, n):
         to = peer(f, j)
         start(remote(active_all.at[f], active_all.at[f], active_ss.at[to], active_rs.at[f], to, t))
-    send_weights(down_copy, DN_A)
-    swap_weights(up_copy, up, up_ss, up_rs)
+    stage(4)
 
     for j in range(1, n + 1):
         at = peer(t, j)
@@ -390,13 +395,14 @@
             copy = remote(mix_send.at[at], mix_recv.at[t], mix_ss.at[at], mix_rs.at[t], f, at)
             copy.start()
             waits.append(copy)
+    stage(5)
     mixed = mix_send[t].astype(f32)
     for j in range(1, n):
         at = peer(t, j)
         remote(mix_send.at[at], mix_recv.at[at], mix_ss.at[at], mix_rs.at[at], f, at).wait_recv()
         mixed = mixed + mix_recv[at].astype(f32)
     summed = residual_scale * normed_all[t].astype(f32) + mixed.astype(bf16).astype(f32)
-    sums, squares = shared_sums(1, summed, "fs", DN_B)
+    sums, squares = shared_sums(1, summed, "fs", 6)
     gain_own = norm_gain[:, pl.ds(pl.multiple_of(f * own_width, 128), own_width)]
     settled_all[t, f] = normalize(summed, sums, squares, width, gain_own).astype(bf16)
 
@@ -407,6 +413,7 @@
 
     for j in range(1, n):
         start(settled_copy(0, t, f, peer(f, j), t, peer(f, j)))
+    stage(7)
     for j in range(n):
         at = peer(f, j)
         if j > 0:
@@ -417,7 +424,7 @@
         at = peer(f, j)
         settled_copy(1, across, at, f, across).wait_recv()
         start(settled_copy(3, across, at, f, mate))
-    swap_weights(down_copy, down, down_ss, down_rs)
+    stage(8)
     for load in loads:
         load.wait()
     swap_wait(up, up_ss, up_rs)
@@ -430,6 +437,7 @@
             hidden[group, h] = jnp.square(jnp.maximum(total, 0.0)).astype(bf16)
 
     make_hidden(t)
+    stage(9)
     for j in range(n):
         at = peer(f, j)
         settled_copy(2, mate, at, f, mate).wait_recv()
@@ -440,6 +448,7 @@
         at = peer(f, j)
         settled_copy(3, opposite, at, f, mate).wait_recv()
     make_hidden(opposite)
+    stage(10)
     swap_wait(down, down_ss, down_rs)
 
     def fed_part(group, block):

time: 145 us -> 131 us (0.903)
  Pallas kernels: 143 us -> 130 us
    pallas_call x1, Pallas kernels: 143 us -> 130 us  [fast_shards(): pl.pallas_call(functools.partial(layer_kernel, n, seq_length), out_shape=...]
where the time goes in v3:
time: 131 us
  Pallas kernels  130 us (99%)
  local copies, waits for them, and re-layouts  1.57 us (1%)
    pallas_call x1, Pallas kernels, fast_shards(): pl.pallas_call(functools.partial(layer_kernel, n, seq_length), out_shape=...  130 us

profile of v3, /device:TPU:0, one launch (start us, length us, event | category | flops | bytes accessed | tf_op | source)
XLA Modules:
  0.0 131.1 jit_solution(11741394572164753795)
XLA Ops:
  0.0 129.6 %shard_map.118 = bf16[128,512]{1,0:T(8,128)(2,1)} custom-call(bf16[128,2048]{1,0:T(8,128)(2,1)} %bitcast.7, f32[1,2048]{1,0:T(1,128)} %bitcast.9, bf16[512,256]{1,0:T(8,128)(2,1)} %value_weight.1, bf16[512,256]{1,0:T(8,128)(2,1)} %gate_weight.1, bf16[31,256]{1,0:T(8,128)(2,1)} %conv_kernel.1, f32[1,256]{1,0:T(1,128)} %bitcast.12, f32[1,256]{1,0:T(1,128)} %bitcast.13, ...), custom_call_target="tpu_custom_call" | custom-call | tf_op jit(solution)/shard_map/pallas_call | solution.py:519
  129.6 1.6 %copy.14 = bf16[1,128,512]{2,1,0:T(8,128)(2,1)} copy(bf16[1,128,512]{2,1,0:T(8,128)(2,1)} %bitcast.8) | data formatting | bytes 262144
